TPU v7x, 32 devices: a whole 2x2x4 slice. The times are simulated.
32 devices in a mesh: sp: 8 (over z, y), tp: 4 (over x, core).
Axes of the slice: x: 2, y: 2, z: 4, core: 2. Of those that a mesh axis runs over, the one named last changes fastest.
Arguments:
- tokens_in: bfloat16 [2048, 2048], P('sp'), may hold values from -6 to 6
- norm_gain: float32 [2048], replicated, may hold values from 0.1 to 1.9
- rec_query_weight: bfloat16 [2048, 1024], P('sp', 'tp'), may hold values from -0.125 to 0.125
- rec_forget_weight: bfloat16 [2048, 1024], P('sp', 'tp'), may hold values from -0.125 to 0.125
- rec_input_weight: bfloat16 [2048, 1024], P('sp', 'tp'), may hold values from -0.125 to 0.125
- att_query_weight: bfloat16 [2048, 1024], P('sp', 'tp'), may hold values from -0.18991481 to 0.18991481
- att_key_weight: bfloat16 [2048, 1024], P('sp', 'tp'), may hold values from -0.18991481 to 0.18991481
- att_value_weight: bfloat16 [2048, 1024], P('sp', 'tp'), may hold values from -0.125 to 0.125
- recurrence_output_weight: bfloat16 [1024, 2048], P('tp'), may hold values from -0.125 to 0.125
- out_att_weight: bfloat16 [1024, 2048], P('tp'), may hold values from -0.125 to 0.125
- floor_gap: float32 [1024], P('tp'), may hold values from 0 to 0.1
- decay_shift: float32 [8, 2048], P('tp', 'sp'), may hold values from -1.5 to 0
- rec_gain: float32 [128], replicated, may hold values from 0.1 to 1.9
- att_gain: float32 [128], replicated, may hold values from 0.1 to 1.9
- lambda_head: float32 [8], P('tp'), may hold values from 0.3 to 0.8
Outputs:
- mixed: bfloat16 [2048, 2048], P('sp')
All inputs are finite; a program needn't handle non-finite values.
Results may differ from a plain program's by a relative error of at most 0.015.
Values may be sent and summed in bfloat16 or wider, within the bound.
A program may use at most 128 MiB of HBM per device.

v0:
```python
import jax
import jax.numpy as jnp
from jax import lax
from jax.sharding import PartitionSpec as P

REC_KEY = 128
REC_VAL = 128
PAIR = 64
ATT_VAL = 128
BLOCK = 64


RECUR_EPSILON = 1e-06
ATTEND_EPSILON = 1e-05
ROTARY_BASE = 10000.0
TOP_PRECISION = lax.Precision.HIGHEST


def prefix_2(array, axis, combine, identity):
    count, position = (lax.axis_size(axis), lax.axis_index(axis))
    everything = jax.tree.map(
        lambda part, kind: lax.all_gather(part.astype(kind), axis),
        array,
        (jnp.bfloat16, jnp.bfloat16),
    )
    start = jax.tree.map(
        lambda part, zero: jnp.broadcast_to(jnp.asarray(zero, part.dtype), part.shape),
        array,
        identity,
    )

    def turn(k, before):
        reached = k < position
        new = combine(
            before, jax.tree.map(lambda part, own: part[k].astype(own.dtype), everything, array)
        )
        return jax.tree.map(lambda a, b: jnp.where(reached, a, b), new, before)

    return lax.fori_loop(0, count, turn, start)


def from_behind(block, axis, distance):
    devices = range(lax.axis_size(axis))
    route = [(i - distance, i) for i in devices if i - distance in devices]
    return lax.ppermute(block, axis, route)


def rms_scale(values, scales, epsilon):
    mean_sq = jnp.mean(values * values, axis=-1, keepdims=True)
    return values * lax.rsqrt(mean_sq + epsilon) * scales


def rotary(values, positions):
    half_width = values.shape[-1] // 2
    frequency = 1.0 / ROTARY_BASE ** (jnp.arange(half_width, dtype=jnp.float32) / half_width)
    angles = positions[:, None] * frequency[None, :]
    cosine = jnp.cos(angles)[:, None, :]
    sine_part = jnp.sin(angles)[:, None, :]
    first_half = values[..., :half_width]
    second_half = values[..., half_width:]
    return jnp.concatenate(
        [
            first_half * cosine - second_half * sine_part,
            second_half * cosine + first_half * sine_part,
        ],
        axis=-1,
    )


def recur_blocks(queries, gate_key_rows, inputs, log_decay, carry_in):
    head_count = queries.shape[0]
    length = queries.shape[1]
    block_count = length // BLOCK

    def split_blocks(array):
        return array.reshape(head_count, block_count, BLOCK, array.shape[-1]).transpose(1, 0, 2, 3)

    causal = jnp.tril(jnp.ones((BLOCK, BLOCK), dtype=bool))

    def advance(carried, bundle):
        q_block, k_block, v_block, g_block = bundle
        cum_log = jnp.cumsum(g_block, axis=1)
        q_decayed = q_block * jnp.exp(cum_log)
        k_growth = k_block * jnp.exp(-cum_log)
        from_past = jnp.einsum("hcd,hde->hce", q_decayed, carried, precision=TOP_PRECISION)
        scores = jnp.einsum("htd,hsd->hts", q_decayed, k_growth, precision=TOP_PRECISION)
        scores = jnp.where(causal[None], scores, 0.0)
        within = jnp.einsum("hts,hse->hte", scores, v_block, precision=TOP_PRECISION)
        end_log = cum_log[:, -1:, :]
        k_to_end = k_block * jnp.exp(end_log - cum_log)
        fresh = jnp.exp(end_log[:, 0, :])[:, :, None] * carried + jnp.einsum(
            "hsd,hse->hde", k_to_end, v_block, precision=TOP_PRECISION
        )
        return (fresh, from_past + within)

    final_state, outputs = lax.scan(
        advance,
        carry_in,
        (
            split_blocks(queries),
            split_blocks(gate_key_rows),
            split_blocks(inputs),
            split_blocks(log_decay),
        ),
    )
    return (
        outputs.transpose(1, 0, 2, 3).reshape(head_count, length, inputs.shape[-1]),
        final_state,
    )


def chain(earlier, latter):
    return (earlier[0] * latter[0], latter[0][:, :, None] * earlier[1] + latter[1])


def absorb(running_total, queries, key_rows, value_rows, allowed):
    best_score, sums_exp, weighted = running_total
    scores = jnp.einsum(
        "qhcd,khcd->hcqk", queries, key_rows, preferred_element_type=jnp.float32
    ) * queries.shape[-1] ** (-0.5)
    scores = jnp.where(allowed, scores, -jnp.inf)
    new_best = jnp.maximum(best_score, jnp.max(scores, axis=-1))
    rescale = jnp.exp(best_score - new_best)
    expo_vals = jnp.exp(scores - new_best[..., None])
    sums_exp = sums_exp * rescale + jnp.sum(expo_vals, axis=-1)
    weighted = weighted * rescale[..., None] + jnp.einsum(
        "hcqk,khe->hcqe",
        expo_vals.astype(jnp.bfloat16),
        value_rows,
        preferred_element_type=jnp.float32,
    )
    return (new_best, sums_exp, weighted)


def per_device(
    tokens_in,
    norm_gain,
    rec_query_weight,
    rec_forget_weight,
    rec_input_weight,
    att_query_weight,
    att_key_weight,
    att_value_weight,
    recurrence_output_weight,
    out_att_weight,
    floor_gap,
    decay_shift,
    rec_gain,
    att_gain,
    lambda_head,
):
    tok_rows = tokens_in.shape[0]
    seq_span = lax.axis_size("sp") // 4
    half_span = seq_span // 2
    dev_index = lax.axis_index("sp")
    first_dev = jnp.maximum(0, (dev_index + half_span) // seq_span * seq_span - half_span)
    carry_on = jnp.where(dev_index == first_dev, 0.0, 1.0).astype(jnp.float32)
    gathered = (
        lax.all_gather(rec_query_weight, "sp", axis=0, tiled=True),
        lax.all_gather(rec_forget_weight, "sp", axis=0, tiled=True),
        lax.all_gather(rec_input_weight, "sp", axis=0, tiled=True),
        lax.all_gather(att_query_weight, "sp", axis=0, tiled=True),
        lax.all_gather(att_key_weight, "sp", axis=0, tiled=True),
        lax.all_gather(att_value_weight, "sp", axis=0, tiled=True),
    )
    w_query, w_forget, w_input, w_att_query, w_att_key, w_att_value = gathered
    normed = rms_scale(tokens_in.astype(jnp.float32), norm_gain, RECUR_EPSILON).astype(jnp.bfloat16)

    def project(weight):
        return jnp.dot(normed, weight, preferred_element_type=jnp.float32)

    rec_query = project(w_query).astype(jnp.bfloat16)
    rec_forget = project(w_forget).astype(jnp.bfloat16)
    rec_input = project(w_input).astype(jnp.bfloat16)
    att_heads = w_att_query.shape[1] // (2 * PAIR)
    positions = ((dev_index - first_dev) * tok_rows + jnp.arange(tok_rows, dtype=jnp.int32)).astype(
        jnp.float32
    )
    att_query = (
        rotary(project(w_att_query).reshape(tok_rows, att_heads * 2, PAIR), positions)
        .astype(jnp.bfloat16)
        .reshape(tok_rows, att_heads, 2, PAIR)
    )
    att_key = (
        rotary(project(w_att_key).reshape(tok_rows, att_heads * 2, PAIR), positions)
        .astype(jnp.bfloat16)
        .reshape(tok_rows, att_heads * 2 * PAIR)
    )
    att_value = project(w_att_value).astype(jnp.bfloat16)
    rec_heads = w_query.shape[1] // REC_KEY
    gate_key = floor_gap[None, :] * jax.nn.sigmoid(-rec_forget.astype(jnp.float32))
    log_decay = (
        jnp.log1p(-gate_key).reshape(tok_rows, rec_heads, REC_KEY) + decay_shift.T[:, :, None]
    )

    def by_head(array, column_count):
        return array.reshape(tok_rows, rec_heads, column_count).transpose(1, 0, 2)

    query_heads = by_head(rec_query.astype(jnp.float32), REC_KEY)
    k_heads = by_head(gate_key, REC_KEY)
    v_heads = by_head(rec_input.astype(jnp.float32), REC_VAL)
    g_heads = log_decay.transpose(1, 0, 2)
    zero_state = jnp.zeros((rec_heads, REC_KEY, REC_VAL), jnp.float32)
    local_out, local_state = recur_blocks(query_heads, k_heads, v_heads, g_heads, zero_state)
    reach_logarithm = jnp.cumsum(g_heads, axis=1)
    span_decay = jnp.exp(reach_logarithm[:, -1, :]) * carry_on
    prefix = prefix_2(
        (span_decay, local_state), "sp", chain, (jnp.ones_like(span_decay), zero_state)
    )
    incoming_state = prefix[1] * carry_on
    rec_raw = local_out + jnp.einsum(
        "ezp,ept->ezt",
        query_heads * jnp.exp(reach_logarithm),
        incoming_state,
        precision=TOP_PRECISION,
    )
    rec_mix = (
        rms_scale(rec_raw.transpose(1, 0, 2), rec_gain, RECUR_EPSILON)
        .astype(jnp.bfloat16)
        .reshape(tok_rows, rec_heads * REC_VAL)
    )
    mask_own = jnp.arange(tok_rows)[:, None] >= jnp.arange(tok_rows)[None, :]
    start_state = (
        jnp.full((att_heads, 2, tok_rows), -jnp.inf, jnp.float32),
        jnp.zeros((att_heads, 2, tok_rows), jnp.float32),
        jnp.zeros((att_heads, 2, tok_rows, ATT_VAL), jnp.float32),
    )
    online = absorb(
        start_state,
        att_query,
        att_key.reshape(tok_rows, att_heads, 2, PAIR),
        att_value.reshape(tok_rows, att_heads, ATT_VAL),
        mask_own,
    )
    everything = jnp.array(True)

    def take_block(state_now, keys_flat, values_flat, source):
        key_rows = keys_flat.reshape(tok_rows, att_heads, 2, PAIR)
        value_rows = values_flat.reshape(tok_rows, att_heads, ATT_VAL)
        return lax.cond(
            source >= first_dev,
            lambda held: absorb(held, att_query, key_rows, value_rows, everything),
            lambda held: held,
            state_now,
        )

    def relay_turn(hop_count, carried):
        moving_keys, moving_values, state_now = carried
        moving_keys, moving_values = from_behind((moving_keys, moving_values), "sp", 1)
        return (
            moving_keys,
            moving_values,
            take_block(state_now, moving_keys, moving_values, dev_index - hop_count - 1),
        )

    online = lax.fori_loop(0, seq_span - 1, relay_turn, (att_key, att_value, online))[2]
    best_score, sums_exp, weighted = online
    att_raw = (
        weighted[:, 0] / sums_exp[:, 0, :, None]
        - lambda_head[:, None, None] * weighted[:, 1] / sums_exp[:, 1, :, None]
    )
    att_mix = (
        rms_scale(att_raw.transpose(1, 0, 2), att_gain, ATTEND_EPSILON)
        .astype(jnp.bfloat16)
        .reshape(tok_rows, att_heads * ATT_VAL)
    )
    partial_value = jnp.dot(rec_mix, recurrence_output_weight, preferred_element_type=jnp.float32)
    partial_value = partial_value + jnp.dot(
        att_mix, out_att_weight, preferred_element_type=jnp.float32
    )
    return lax.psum(partial_value.astype(jnp.bfloat16), "tp")


def solution(mesh):
    in_specs = (
        P("sp", None),
        P(),
        P("sp", "tp"),
        P("sp", "tp"),
        P("sp", "tp"),
        P("sp", "tp"),
        P("sp", "tp"),
        P("sp", "tp"),
        P("tp", None),
        P("tp", None),
        P("tp"),
        P("tp", "sp"),
        P(),
        P(),
        P("tp"),
    )
    out_specs = P("sp", None)
    return jax.shard_map(
        per_device, mesh=mesh, in_specs=in_specs, out_specs=out_specs, check_vma=False
    )
```

profile of v0, /device:TPU:25, one launch (start us, length us, event | category | flops | bytes accessed | tf_op | source)
XLA Modules:
  0.0 356.3 jit_solution(13360508003961837812)
XLA Ops:
  11.2 1.5 fusion.30
  13.0 34.4 %all-gather.15.cloned.1.call-done = bf16[2048,256]{1,0:T(8,128)(2,1)} async-done(((bf16[256,256]{1,0:T(8,128)(2,1)}), bf16[2048,256]{1,0:T(8,128)(2,1)}) %all-gather.15.cloned.1.call-update) | async-done | bytes 1048592 | tf_op jit(solution)/shard_map/all_gather | solution.py:162
  47.4 2.2 fusion.64
  49.6 38.9 %all-gather.17.cloned.1.call-done = bf16[2048,256]{1,0:T(8,128)(2,1)} async-done(((bf16[256,256]{1,0:T(8,128)(2,1)}), bf16[2048,256]{1,0:T(8,128)(2,1)}) %all-gather.17.cloned.1.call-update) | async-done | bytes 1048592 | tf_op jit(solution)/shard_map/all_gather | solution.py:163
  88.6 1.9 fusion.62
  91.3 2.4 collective-permute-start
  93.6 36.1 %all-gather.19.cloned.1.call-done = bf16[2048,256]{1,0:T(8,128)(2,1)} async-done(((bf16[256,256]{1,0:T(8,128)(2,1)}), bf16[2048,256]{1,0:T(8,128)(2,1)}) %all-gather.19.cloned.1.call-update) | async-done | bytes 1048592 | tf_op jit(solution)/shard_map/all_gather | solution.py:164
  129.7 2.5 convolution_convert_fusion
  132.3 2.5 collective-permute-start.1
  134.8 35.9 %all-gather.9.cloned.1.call-done = bf16[2048,256]{1,0:T(8,128)(2,1)} async-done(((bf16[256,256]{1,0:T(8,128)(2,1)}), bf16[2048,256]{1,0:T(8,128)(2,1)}) %all-gather.9.cloned.1.call-update) | async-done | bytes 1048592 | tf_op jit(solution)/shard_map/all_gather | solution.py:160
  170.7 2.7 negate_log-plus-one_fusion
  174.1 12.1 %all-gather = bf16[16,1,128]{2,1,0:T(2,128)(2,1)S(1)} all-gather(bf16[2,1,128]{2,1,0:T(2,128)(2,1)S(1)} %fusion.58), channel_id=2, replica_groups=mesh['sp'=8,'tp'=4] {'sp'}, dimensions={0}, use_global_device_ids=true | all-gather | bytes 4608 | tf_op jit(solution)/shard_map/all_gather | solution.py:22
  186.2 1.1 copy.48
  187.3 24.4 %all-gather.13.cloned.1.call-done = bf16[2048,256]{1,0:T(8,128)(2,1)} async-done(((bf16[256,256]{1,0:T(8,128)(2,1)}), bf16[2048,256]{1,0:T(8,128)(2,1)}) %all-gather.13.cloned.1.call-update) | async-done | bytes 1048592 | tf_op jit(solution)/shard_map/all_gather | solution.py:159
  211.7 2.5 convolution_convert_fusion.1
  214.3 1.0 copy.50
  215.3 1.3 fusion.72
  217.7 35.0 %all-gather.11.cloned.1.call-done = bf16[2048,256]{1,0:T(8,128)(2,1)} async-done(((bf16[256,256]{1,0:T(8,128)(2,1)}), bf16[2048,256]{1,0:T(8,128)(2,1)}) %all-gather.11.cloned.1.call-update) | async-done | bytes 1048592 | tf_op jit(solution)/shard_map/all_gather | solution.py:161
  252.7 2.6 convolution_convert_fusion.2
  255.3 1.0 copy.49
  256.3 7.7 %while.8 = (s32[]{:T(128)}, f32[2,128,128]{2,1,0:T(8,128)S(1)}, f32[4,2,64,128]{3,2,0,1:T(8,128)}, f32[4,2,64,128]{3,2,0,1:T(8,128)S(1)}, f32[4,2,64,128]{3,2,0,...) while((s32[]{:T(128)}, f32[2,128,128]{2,1,0:T(8,128)S(1)}, ...), condition=%wide.region_3.4_spmd.clone, body=%wide.region_1.3_spmd.clone.sunk | while | flops 76787712 | bytes 1627260 | solution.py:96
  264.0 24.4 %all-gather.1 = bf16[16,128,128]{2,1,0:T(8,128)(2,1)S(1)} all-gather(bf16[2,128,128]{2,1,0:T(8,128)(2,1)S(1)} %convert_element_type.106), channel_id=3, replica_groups=mesh['sp'=8,'tp'=4] {'sp'}, dimensions={0}, use_global_device_ids=true | all-gather | bytes 589824 | tf_op jit(solution)/shard_map/all_gather | solution.py:22
  288.4 1.4 while.18
  291.6 2.1 convolution_add_fusion.4
  293.8 3.8 %conditional.1 = ((f32[2,2,256]{2,1,0:T(2,128)S(1)}, f32[2,2,256,128]{3,2,1,0:T(8,128)})) conditional(s32[]{:T(128)} %convert_element_type.108, (f32[2,2,256]{2,1,0:T(2,128)S(1)}, f32[2,2,256,128]{3,2,1,0:T(8,128)}) %tuple.39, (bf16[256,256]{0,1:T(8,128)(2,1)}, bf16[256,2,2,64]{0,3,2,1:T(8,128)(2,1)S(1)}, f32[2,2,256]{2,1,0:T(2,128)S(1)}, ...), branch_computations={%region_11.12_spmd, %region_12.15_spmd} | conditional | flops 102500352 | bytes 8839248 | solution.py:240
  293.8 1.3 fusion.70
  295.4 1.4 convolution_add_fusion
  297.6 2.0 copy.63
  299.6 1.2 multiply_reduce_fusion
  300.9 2.7 fusion.29
  303.6 43.6 %all-reduce.2.cloned.1.call-done = bf16[256,2048]{1,0:T(8,128)(2,1)} async-done(((bf16[256,2048]{1,0:T(8,128)(2,1)}), bf16[256,2048]{1,0:T(8,128)(2,1)}) %all-reduce.2.cloned.1.call-update) | async-done | bytes 1048592 | tf_op jit(solution)/shard_map/psum | solution.py:271
  347.1 2.3 copy.117
  (136 shorter events, 18.8 us)
Async XLA Ops:
  6.5 284.0 %copy-start = (bf16[256,2048]{1,0:T(8,128)(2,1)S(1)}, bf16[256,2048]{1,0:T(8,128)(2,1)}, u32[]{:S(2)}) copy-start(bf16[256,2048]{1,0:T(8,128)(2,1)} %param.29) | copy-start | bytes 3145732
  6.5 40.9 %all-gather.15.cloned.1.call-start = ((), (), s32[]{:S(2)}) async-start(), calls=%async_computation.3 | async-start | bytes 1179648 | tf_op jit(solution)/shard_map/all_gather | solution.py:162
  7.3 81.3 %all-gather.17.cloned.1.call-start = ((), (), s32[]{:S(2)}) async-start(), calls=%async_computation.4 | async-start | bytes 1179648 | tf_op jit(solution)/shard_map/all_gather | solution.py:163
  8.0 121.7 %all-gather.19.cloned.1.call-start = ((), (), s32[]{:S(2)}) async-start(), calls=%async_computation.5 | async-start | bytes 1179648 | tf_op jit(solution)/shard_map/all_gather | solution.py:164
  8.7 162.0 %all-gather.9.cloned.1.call-start = ((), (), s32[]{:S(2)}) async-start(), calls=%async_computation | async-start | bytes 1179648 | tf_op jit(solution)/shard_map/all_gather | solution.py:160
  9.3 202.4 %all-gather.13.cloned.1.call-start = ((), (), s32[]{:S(2)}) async-start(), calls=%async_computation.2 | async-start | bytes 1179648 | tf_op jit(solution)/shard_map/all_gather | solution.py:159
  9.9 242.8 %all-gather.11.cloned.1.call-start = ((), (), s32[]{:S(2)}) async-start(), calls=%async_computation.1 | async-start | bytes 1179648 | tf_op jit(solution)/shard_map/all_gather | solution.py:161
  10.5 78.1 %copy-start.5 = (bf16[256,2048]{1,0:T(8,128)(2,1)S(1)}, bf16[256,2048]{1,0:T(8,128)(2,1)}, u32[]{:S(2)}) copy-start(bf16[256,2048]{1,0:T(8,128)(2,1)} %param.21) | copy-start | bytes 3145732
  10.5 78.1 %copy-start.14 = (f32[2048]{0:T(1024)S(1)}, f32[2048]{0:T(1024)}, u32[]{:S(2)}) copy-start(f32[2048]{0:T(1024)} %param.22) | copy-start | bytes 24580
  10.5 336.6 %all-reduce.2.cloned.1.call-start = ((), (), s32[]{:S(2)}) async-start(), calls=%async_computation.6 | async-start | bytes 2097152 | tf_op jit(solution)/shard_map/psum | solution.py:271
  12.8 199.0 %copy-start.10 = (f32[256]{0:T(256)}, f32[256]{0:T(256)S(1)}, u32[]{:S(2)}) copy-start(f32[256]{0:T(256)S(1)} %add_rsqrt_fusion.2) | copy-start | bytes 3076
  90.5 80.3 %copy-start.15 = (f32[256]{0:T(256)S(1)}, f32[256]{0:T(256)}, u32[]{:S(2)}) copy-start(f32[256]{0:T(256)} %param.31) | copy-start | bytes 3076
  90.5 44.2 %copy-start.7 = (bf16[256,4,32]{0,2,1:T(8,128)(2,1)}, bf16[256,4,32]{0,2,1:T(8,128)(2,1)S(1)}, u32[]{:S(2)}) copy-start(bf16[256,4,32]{0,2,1:T(8,128)(2,1)S(1)} %get-tuple-element.328) | copy-start | bytes 196612
  90.6 44.2 %copy-start.8 = (bf16[256,4,32]{0,2,1:T(8,128)(2,1)}, bf16[256,4,32]{0,2,1:T(8,128)(2,1)S(1)}, u32[]{:S(2)}) copy-start(bf16[256,4,32]{0,2,1:T(8,128)(2,1)S(1)} %get-tuple-element.329) | copy-start | bytes 196612
  91.3 202.5 %collective-permute-start = (bf16[256,256]{0,1:T(8,128)(2,1)}, bf16[256,256]{0,1:T(8,128)(2,1)}, u32[]{:S(2)}, u32[]{:S(2)}) collective-permute-start(bf16[256,256]{0,1:T(8,128)(2,1)} %bitcast.39), channel_id=1, source_target_pairs={{0,4},{4,8},{8,12},{12,16},{16,20},{20,24},{24,28},{1,5},{5,9},{9,... | collective-permute-start | bytes 393224 | tf_op jit(solution)/shard_map/while/body/eval_jaxpr/ppermute | solution.py:45
  132.3 41.2 %copy-start.9 = (f32[2,256]{1,0:T(2,128)S(1)}, f32[2,256]{1,0:T(2,128)}, u32[]{:S(2)}) copy-start(f32[2,256]{1,0:T(2,128)} %param.32) | copy-start | bytes 6148
  132.3 161.5 %collective-permute-start.1 = (bf16[256,256]{0,1:T(8,128)(2,1)}, bf16[256,256]{0,1:T(8,128)(2,1)}, u32[]{:S(2)}, u32[]{:S(2)}) collective-permute-start(bf16[256,256]{0,1:T(8,128)(2,1)} %convolution_convert_fusion), channel_id=1, source_target_pairs={{0,4},{4,8},{8,12},{12,16},{16,20},{20,24},{24,28},{1,5},{5,9},{9,... | collective-permute-start | bytes 393224 | tf_op jit(solution)/shard_map/while/body/eval_jaxpr/ppermute | solution.py:45
  216.6 1.0 copy-start.3
  264.0 25.8 %copy-start.6 = (f32[4,2,64,128]{3,2,0,1:T(8,128)S(1)}, f32[4,2,64,128]{3,2,0,1:T(8,128)}, u32[]{:S(2)}) copy-start(f32[4,2,64,128]{3,2,0,1:T(8,128)} %get-tuple-element.213) | copy-start | bytes 786436
  264.0 26.4 %copy-start.11 = (f32[128]{0:T(128)S(1)}, f32[128]{0:T(128)}, u32[]{:S(2)}) copy-start(f32[128]{0:T(128)} %param.33) | copy-start | bytes 1540
  290.4 1.2 copy-start.4
  293.8 5.8 %copy-start.13 = (f32[2]{0:T(128)S(1)}, f32[2]{0:T(128)}, u32[]{:S(2)}) copy-start(f32[2]{0:T(128)} %param.35) | copy-start | bytes 28
  293.8 7.0 %copy-start.12 = (f32[128]{0:T(128)S(1)}, f32[128]{0:T(128)}, u32[]{:S(2)}) copy-start(f32[128]{0:T(128)} %param.34) | copy-start | bytes 1540
  293.8 1.5 copy-start.1
  296.8 0.8 copy-start.2
Sparse Core Ops, SparseCore 0:
  9.5 37.9 all-gather.14
  49.5 38.9 all-gather.16
  90.7 38.9 all-gather.18
  131.7 38.9 all-gather.8
  172.7 38.9 all-gather.12
  213.7 38.9 all-gather.10
  303.7 43.3 all-reduce.1
where the time goes:
time: 359 us; the launch traced here: 356 us
  waiting for transfers between devices  252 us (70%)
  blocking collectives  36.6 us (10%)
  matrix products  31 us (9%)
  between operations  13.9 us (4%)
  local copies, waits for them, and re-layouts  10.3 us (3%)
  other arithmetic  6.92 us (2%)
  starting transfers between devices  5.07 us (1%)
    psum x1, waiting for transfers between devices, per_device(): return lax.psum(partial_value.astype(jnp.bfloat16), 'tp')  43.6 us
    all_gather x1, waiting for transfers between devices, per_device(): lax.all_gather(att_key_weight, 'sp', axis=0, tiled=True)  38.9 us
    all_gather x2, blocking collectives, prefix_2(): lax.all_gather(part.astype(kind), axis)  36.6 us
    all_gather x1, waiting for transfers between devices, per_device(): lax.all_gather(att_value_weight, 'sp', axis=0, tiled=True)  36.1 us
    all_gather x1, waiting for transfers between devices, per_device(): lax.all_gather(rec_forget_weight, 'sp', axis=0, tiled=True)  35.9 us
    all_gather x1, waiting for transfers between devices, per_device(): lax.all_gather(rec_input_weight, 'sp', axis=0, tiled=True)  35 us
    all_gather x1, waiting for transfers between devices, per_device(): lax.all_gather(att_query_weight, 'sp', axis=0, tiled=True)  34.4 us
    all_gather x1, waiting for transfers between devices, per_device(): lax.all_gather(rec_query_weight, 'sp', axis=0, tiled=True)  24.4 us
  transfers between devices with their start and end apart: 9, of which 7 were waited for; matrix products, arithmetic and copies ran while one was open for 10% of the time, Pallas kernels for 0%

commit v1 on v0

--- a/solution.py
+++ b/solution.py
@@ -1,6 +1,10 @@
+import functools
+
 import jax
 import jax.numpy as jnp
 from jax import lax
+from jax.experimental import pallas as pl
+from jax.experimental.pallas import tpu as pltpu
 from jax.sharding import PartitionSpec as P
 
 REC_KEY = 128
@@ -271,6 +275,398 @@
     return lax.psum(partial_value.astype(jnp.bfloat16), "tp")
 
 
+MESH = pl.DeviceIdType.MESH
+F32 = jnp.float32
+BF16 = jnp.bfloat16
+CUT = 128
+
+
+def nt(a, b):
+    return lax.dot_general(a, b, (((1,), (1,)), ((), ())), preferred_element_type=F32)
+
+
+def tn(a, b):
+    return lax.dot_general(a, b, (((0,), (0,)), ((), ())), preferred_element_type=F32)
+
+
+def nn(a, b):
+    return jnp.dot(a, b, preferred_element_type=F32)
+
+
+def halves(x):
+    high = x.astype(BF16)
+    return high, (x - high.astype(F32)).astype(BF16)
+
+
+def turn_map(values, cosine, sine_part):
+    width = values.shape[-1]
+    lane = lax.broadcasted_iota(jnp.int32, values.shape, 1)
+    ahead = pltpu.roll(values, width - PAIR // 2, 1)
+    back = pltpu.roll(values, PAIR // 2, 1)
+    other = jnp.where(lane % PAIR < PAIR // 2, ahead, back)
+    return values * cosine + other * sine_part
+
+
+def fused_kernel(
+    n, tps, span,
+    tokens, gain, wk, wv, wq, wf, wi, wr, rec_out, att_out, gap, shift, rec_gain, att_gain, cosine, sine_part,
+    lam, out,
+    buf, xn, acc, wo, mix, kv, kv_prev, st, st_prev, total,
+    ssem, rsem, wo_s, wo_r, mix_s, mix_r, ex_s, ex_r,
+):
+    weights = (wk, wv, wq, wf, wi, wr)
+    chunks = len(weights)
+    rows, width = tokens.shape
+    depth, cols = wk.shape
+    me = lax.axis_index("sp")
+    t = lax.axis_index("tp")
+    up = (1 - me % 2)
+    place = up * (me // 2) + (1 - up) * (n - 1 - me // 2)
+
+    def at_place(p):
+        q = (p + n) % n
+        low = q // (n // 2)
+        return (1 - low) * (2 * q) + low * (2 * (n - 1 - q) + 1)
+
+    right, left = at_place(place + 1), at_place(place - 1)
+    partner = t + 1 - 2 * (t % 2)
+    across = (t + 2) % tps
+    half = span // 2
+    stage = (me + half) % span
+    is_recv = jnp.logical_and(stage > 0, me >= half)
+    is_send = jnp.logical_and(stage == 0, me + 1 < n)
+    to_right, to_left = {"sp": right}, {"sp": left}
+    to_partner, to_across = {"tp": partner}, {"tp": across}
+
+    barrier = pltpu.get_barrier_semaphore()
+    for target in (to_right, to_left, to_partner, to_across):
+        pl.semaphore_signal(barrier, inc=1, device_id=target, device_id_type=MESH)
+
+    @pl.when(is_send)
+    def _():
+        pl.semaphore_signal(barrier, inc=1, device_id={"sp": me + 1}, device_id_type=MESH)
+
+    @pl.when(is_recv)
+    def _():
+        pl.semaphore_signal(barrier, inc=1, device_id={"sp": me - 1}, device_id_type=MESH)
+
+    paired = jnp.logical_or(is_send, is_recv)
+
+    @pl.when(paired)
+    def _():
+        pl.semaphore_wait(barrier, 5)
+
+    @pl.when(jnp.logical_not(paired))
+    def _():
+        pl.semaphore_wait(barrier, 4)
+
+    top = n // 2
+
+    def slot(way, hop):
+        return hop if way == 0 else n - hop
+
+    def carried(way, hop):
+        if hop < top:
+            return tuple(range(chunks))
+        if hop == top:
+            return tuple(range(chunks // 2)) if way == 0 else tuple(range(chunks // 2, chunks))
+        return ()
+
+    def ring(way, hop, c):
+        return pltpu.make_async_remote_copy(
+            src_ref=weights[c] if hop == 1 else buf.at[slot(way, hop - 1), c],
+            dst_ref=buf.at[slot(way, hop), c],
+            send_sem=ssem.at[way, hop - 1, c],
+            recv_sem=rsem.at[slot(way, hop), c],
+            device_id=(to_right, to_left)[way],
+            device_id_type=MESH,
+        )
+
+    def remote(src, dst, s, r, target):
+        return pltpu.make_async_remote_copy(
+            src_ref=src, dst_ref=dst, send_sem=s, recv_sem=r, device_id=target, device_id_type=MESH
+        )
+
+    outs_w = (rec_out, att_out)
+
+    def wo_copy(k, part):
+        src = outs_w[part] if k < 2 else wo.at[1, part]
+        return remote(src, wo.at[k, part], wo_s.at[k, part], wo_r.at[k, part], to_across if k == 1 else to_partner)
+
+    def mix_copy(k, part):
+        src = mix.at[3, part] if k < 2 else mix.at[1, part]
+        return remote(src, mix.at[k, part], mix_s.at[k, part], mix_r.at[k, part], to_across if k == 1 else to_partner)
+
+    for c in range(chunks):
+        for way in range(2):
+            ring(way, 1, c).start()
+    for part in range(2):
+        wo_copy(1, part).start()
+        wo_copy(0, part).start()
+
+    values = tokens[...].astype(F32)
+    mean_sq = jnp.mean(values * values, axis=-1, keepdims=True)
+    normed = (values * lax.rsqrt(mean_sq + RECUR_EPSILON) * gain[...]).astype(BF16)
+    for k in range(n):
+        xn[k] = normed[:, k * depth : (k + 1) * depth]
+    mine = xn[me]
+    for c in range(chunks):
+        acc[c] = nn(mine, weights[c][...])
+
+    def project(way, hop, c):
+        ring(way, hop, c).wait_recv()
+        if c in carried(way, hop + 1):
+            ring(way, hop + 1, c).start()
+        origin = at_place(place - hop if way == 0 else place + hop)
+        acc[c] = acc[c] + nn(xn[origin], buf[slot(way, hop), c])
+
+    for hop in range(1, top):
+        for c in range(chunks):
+            for way in range(2):
+                project(way, hop, c)
+    for part in range(2):
+        wo_copy(1, part).wait_recv()
+        wo_copy(2, part).start()
+
+    @pl.when(jnp.logical_not(is_recv))
+    def _():
+        kv_prev[...] = jnp.zeros(kv_prev.shape, BF16)
+        st_prev[...] = jnp.zeros(st_prev.shape, F32)
+
+    def ex_copy(k):
+        src, dst = ((kv.at[0], kv_prev.at[0]), (kv.at[1], kv_prev.at[1]), (st, st_prev))[k]
+        return remote(src, dst, ex_s.at[k], ex_r.at[k], {"sp": me + 1})
+
+    heads = cols // CUT
+    blocks = rows // CUT
+    r_iota = lax.broadcasted_iota(jnp.int32, (CUT, CUT), 0)
+    c_iota = lax.broadcasted_iota(jnp.int32, (CUT, CUT), 1)
+    lower = r_iota >= c_iota
+    ones = jnp.where(lower, 1.0, 0.0).astype(BF16)
+
+    project(0, top, 0)
+    for h in range(heads):
+        lanes = slice(h * CUT, (h + 1) * CUT)
+        kv[0, :, lanes] = turn_map(acc[0, :, lanes], cosine[...], sine_part[...]).astype(BF16)
+
+    @pl.when(is_send)
+    def _():
+        ex_copy(0).start()
+
+    project(1, top, 3)
+    cums, keys = [], []
+    for h in range(heads):
+        lanes = slice(h * CUT, (h + 1) * CUT)
+        forget = acc[3, :, lanes].astype(BF16).astype(F32)
+        key = gap[:, lanes] * (1.0 / (1.0 + jnp.exp(forget)))
+        high, low = halves(jnp.log(1.0 - key))
+        for b in range(blocks):
+            part = slice(b * CUT, (b + 1) * CUT)
+            s_high, s_low = halves(jnp.broadcast_to(shift[h : h + 1, part], (CUT, CUT)))
+            cums.append(nn(ones, high[part]) + nn(ones, low[part]) + nt(ones, s_high) + nt(ones, s_low))
+            keys.append(key[part])
+
+    project(0, top, 1)
+    kv[1] = acc[1].astype(BF16)
+
+    @pl.when(is_send)
+    def _():
+        ex_copy(1).start()
+
+    project(1, top, 4)
+    fresh, inputs = [], []
+    for h in range(heads):
+        lanes = slice(h * CUT, (h + 1) * CUT)
+        own = jnp.zeros((CUT, CUT), F32)
+        for b in range(blocks):
+            i = h * blocks + b
+            inp = acc[4, b * CUT : (b + 1) * CUT, lanes].astype(BF16)
+            end = cums[i][CUT - 1 : CUT]
+            to_end = (keys[i] * jnp.exp(end - cums[i])).astype(BF16)
+            fresh.append(own)
+            own = own * jnp.exp(end) + tn(inp, to_end)
+            inputs.append(inp)
+        st[h] = own
+
+    @pl.when(is_send)
+    def _():
+        ex_copy(2).start()
+
+    project(0, top, 2)
+    project(1, top, 5)
+
+    raws, pasts = [], []
+    for h in range(heads):
+        lanes = slice(h * CUT, (h + 1) * CUT)
+        decay = jnp.zeros((1, CUT), F32)
+        for b in range(blocks):
+            i = h * blocks + b
+            cum = cums[i]
+            middle = cum[CUT // 2 - 1 : CUT // 2]
+            q = acc[5, b * CUT : (b + 1) * CUT, lanes].astype(BF16).astype(F32)
+            scores = nt((q * jnp.exp(cum - middle)).astype(BF16), (keys[i] * jnp.exp(middle - cum)).astype(BF16))
+            scores = jnp.where(lower, scores, 0.0).astype(BF16)
+            past = q * jnp.exp(cum)
+            raw = nn(scores, inputs[i])
+            if b:
+                raw = raw + nt(past.astype(BF16), fresh[i].astype(BF16))
+            raws.append(raw)
+            pasts.append((past, decay))
+            decay = decay + cum[CUT - 1 : CUT]
+
+    for part in range(2):
+        wo_copy(0, part).wait_recv()
+        wo_copy(2, part).wait_recv()
+
+    lane = lax.broadcasted_iota(jnp.int32, (rows, CUT), 1)
+    own_mask = lax.broadcasted_iota(jnp.int32, (rows, rows), 0) >= lax.broadcasted_iota(jnp.int32, (rows, rows), 1)
+    away = jnp.where(is_recv, 0.0, -1e30).astype(F32)
+
+    own_scores = []
+    turned = []
+    for h in range(heads):
+        lanes = slice(h * CUT, (h + 1) * CUT)
+        query = turn_map(acc[2, :, lanes], cosine[...], sine_part[...]).astype(BF16)
+        for c in range(2):
+            picked = jnp.where((lane // PAIR) == c, query, jnp.zeros_like(query))
+            turned.append(picked)
+
+    @pl.when(is_recv)
+    def _():
+        for k in range(3):
+            ex_copy(k).wait_recv()
+
+    for h in range(heads):
+        lanes = slice(h * CUT, (h + 1) * CUT)
+        for b in range(blocks):
+            i = h * blocks + b
+            past, decay = pasts[i]
+            came = (st_prev[h] * jnp.exp(decay)).astype(BF16)
+            raw = raws[i] + nt(past.astype(BF16), came)
+            mean_sq = jnp.mean(raw * raw, axis=-1, keepdims=True)
+            mix[3, 0, b * CUT : (b + 1) * CUT, lanes] = (
+                raw * lax.rsqrt(mean_sq + RECUR_EPSILON) * rec_gain[...]
+            ).astype(BF16)
+    mix_copy(1, 0).start()
+    mix_copy(0, 0).start()
+
+    for h in range(heads):
+        lanes = slice(h * CUT, (h + 1) * CUT)
+        found = []
+        for c in range(2):
+            picked = turned[h * 2 + c]
+            s_own = jnp.where(own_mask, nt(picked, kv[0, :, lanes]) * PAIR ** (-0.5), -1e30)
+            s_prev = nt(picked, kv_prev[0, :, lanes]) * PAIR ** (-0.5) + away
+            best = jnp.maximum(jnp.max(s_own, axis=-1, keepdims=True), jnp.max(s_prev, axis=-1, keepdims=True))
+            e_own, e_prev = jnp.exp(s_own - best), jnp.exp(s_prev - best)
+            sums = jnp.sum(e_own, axis=-1, keepdims=True) + jnp.sum(e_prev, axis=-1, keepdims=True)
+            weighted = nn(e_own.astype(BF16), kv[1, :, lanes]) + nn(e_prev.astype(BF16), kv_prev[1, :, lanes])
+            found.append(weighted / sums)
+        raw = found[0] - lam[h] * found[1]
+        mean_sq = jnp.mean(raw * raw, axis=-1, keepdims=True)
+        mix[3, 1, :, lanes] = (raw * lax.rsqrt(mean_sq + ATTEND_EPSILON) * att_gain[...]).astype(BF16)
+    mix_copy(1, 1).start()
+    mix_copy(0, 1).start()
+
+    tile = 2 * cols
+    tiles = width // tile
+
+    def add(k, part, first=False):
+        source = outs_w[part] if k == 3 else wo.at[k, part]
+        left_side = mix[k, part]
+        for j in range(tiles):
+            span_cols = slice(j * tile, (j + 1) * tile)
+            product = nn(left_side, source[:, span_cols])
+            total[:, span_cols] = product if first else total[:, span_cols] + product
+
+    add(3, 0, True)
+    mix_copy(1, 0).wait_recv()
+    mix_copy(2, 0).start()
+    add(3, 1)
+    mix_copy(0, 0).wait_recv()
+    add(0, 0)
+    add(1, 0)
+    mix_copy(2, 0).wait_recv()
+    add(2, 0)
+    mix_copy(0, 1).wait_recv()
+    add(0, 1)
+    mix_copy(1, 1).wait_recv()
+    mix_copy(2, 1).start()
+    add(1, 1)
+    mix_copy(2, 1).wait_recv()
+    left_side = mix[2, 1]
+    for j in range(tiles):
+        span_cols = slice(j * tile, (j + 1) * tile)
+        out[:, span_cols] = (total[:, span_cols] + nn(left_side, wo[2, 1, :, span_cols])).astype(BF16)
+
+    for hop in range(1, top + 1):
+        for way in range(2):
+            for c in carried(way, hop):
+                ring(way, hop, c).wait_send()
+    for k in range(3):
+        for part in range(2):
+            wo_copy(k, part).wait_send()
+            mix_copy(k, part).wait_send()
+
+    @pl.when(is_send)
+    def _():
+        for k in range(3):
+            ex_copy(k).wait_send()
+
+
+def per_device_fused(
+    n, tps, span,
+    tokens_in, norm_gain, rec_query_weight, rec_forget_weight, rec_input_weight,
+    att_query_weight, att_key_weight, att_value_weight, recurrence_output_weight, out_att_weight,
+    floor_gap, decay_shift, rec_gain, att_gain, lambda_head,
+):
+    rows, width = tokens_in.shape
+    depth, cols = att_key_weight.shape
+    me = lax.axis_index("sp")
+    half = span // 2
+    first_dev = jnp.maximum(0, (me + half) // span * span - half)
+    positions = ((me - first_dev) * rows + jnp.arange(rows, dtype=jnp.int32)).astype(F32)
+    half_width = PAIR // 2
+    frequency = 1.0 / ROTARY_BASE ** (jnp.arange(half_width, dtype=F32) / half_width)
+    angles = positions[:, None] * frequency[None, :]
+    cosine = jnp.tile(jnp.cos(angles), (1, 4))
+    sine_one = jnp.sin(angles)
+    sine_part = jnp.concatenate([-sine_one, sine_one, -sine_one, sine_one], axis=1)
+    heads = cols // CUT
+    vmem = pl.BlockSpec(memory_space=pltpu.VMEM)
+    return pl.pallas_call(
+        functools.partial(fused_kernel, n, tps, span),
+        out_shape=jax.ShapeDtypeStruct((rows, width), BF16),
+        in_specs=[vmem] * 16 + [pl.BlockSpec(memory_space=pltpu.SMEM)],
+        out_specs=vmem,
+        scratch_shapes=[
+            pltpu.VMEM((n, 6, depth, cols), BF16),
+            pltpu.VMEM((n, rows, depth), BF16),
+            pltpu.VMEM((6, rows, cols), F32),
+            pltpu.VMEM((3, 2, cols, width), BF16),
+            pltpu.VMEM((4, 2, rows, cols), BF16),
+            pltpu.VMEM((2, rows, cols), BF16),
+            pltpu.VMEM((2, rows, cols), BF16),
+            pltpu.VMEM((heads, CUT, CUT), F32),
+            pltpu.VMEM((heads, CUT, CUT), F32),
+            pltpu.VMEM((rows, width), F32),
+            pltpu.SemaphoreType.DMA((2, n // 2, 6)),
+            pltpu.SemaphoreType.DMA((n, 6)),
+            pltpu.SemaphoreType.DMA((3, 2)),
+            pltpu.SemaphoreType.DMA((3, 2)),
+            pltpu.SemaphoreType.DMA((3, 2)),
+            pltpu.SemaphoreType.DMA((3, 2)),
+            pltpu.SemaphoreType.DMA((3,)),
+            pltpu.SemaphoreType.DMA((3,)),
+        ],
+        compiler_params=pltpu.CompilerParams(collective_id=0, has_side_effects=True, vmem_limit_bytes=56 << 20),
+    )(
+        tokens_in, norm_gain[None], att_key_weight, att_value_weight, att_query_weight,
+        rec_forget_weight, rec_input_weight, rec_query_weight, recurrence_output_weight, out_att_weight,
+        floor_gap[None], decay_shift, rec_gain[None], att_gain[None], cosine, sine_part, lambda_head,
+    )
+
+
 def solution(mesh):
     in_specs = (
         P("sp", None),
@@ -290,6 +686,11 @@
         P("tp"),
     )
     out_specs = P("sp", None)
+    n, tps = mesh.shape["sp"], mesh.shape["tp"]
+    span = n // 4
+    chosen = per_device
+    if span == 2 and tps == 4:
+        chosen = functools.partial(per_device_fused, n, tps, span)
     return jax.shard_map(
-        per_device, mesh=mesh, in_specs=in_specs, out_specs=out_specs, check_vma=False
-    )
+        chosen, mesh=mesh, in_specs=in_specs, out_specs=out_specs, check_vma=False
+    )

time: 359 us -> 89.5 us (0.25)
  waiting for transfers between devices: 252 us -> 0 us
  Pallas kernels: 0 us -> 84.8 us
  blocking collectives: 36.6 us -> 0 us
  matrix products: 31 us -> 0 us
  between operations: 13.9 us -> 0.03 us
  local copies, waits for them, and re-layouts: 10.3 us -> 3.14 us
  other arithmetic: 6.92 us -> 1.38 us
  starting transfers between devices: 5.07 us -> 0 us
    all_gather x6 -> x0, waiting for transfers between devices: 205 us -> none  [the longest x1 38.9 us: per_device(): lax.all_gather(att_key_weight, 'sp', axis=0, tiled=True)]
    pallas_call x0 -> x1, Pallas kernels: none -> 84.8 us  [per_device_fused(): pl.pallas_call(functools.partial(fused_kernel, n, tps, span), out_shape=j...]
    psum x1 -> x0, waiting for transfers between devices: 43.6 us -> none  [per_device(): return lax.psum(partial_value.astype(jnp.bfloat16), 'tp')]
    all_gather x2 -> x0, blocking collectives: 36.6 us -> none  [prefix_2(): lax.all_gather(part.astype(kind), axis)]
    dot_general x29 -> x0, matrix products: 31 us -> none  [the longest x6 14.4 us: project(): return jnp.dot(normed, weight, preferred_element_type=jnp.float32)]
    ppermute x2 -> x0, starting transfers between devices: 4.84 us -> none  [from_behind(): return lax.ppermute(block, axis, route)]
    unnamed x7 -> x0, waiting for transfers between devices: 3.68 us -> none
  transfers between devices with their start and end apart: 9 -> 0, of which waited for: 7 -> 0; matrix products, arithmetic and copies ran while one was open for 10% -> 0% of each run, Pallas kernels for 0% -> 0%
where the time goes in v1:
time: 89.5 us; the launch traced here: 89.3 us
  Pallas kernels  84.8 us (95%)
  local copies, waits for them, and re-layouts  3.14 us (4%)
  other arithmetic  1.38 us (2%)
    pallas_call x1, Pallas kernels, per_device_fused(): pl.pallas_call(functools.partial(fused_kernel, n, tps, span), out_shape=j...  84.8 us
    unnamed x1, local copies, waits for them, and re-layouts  2.3 us

profile of v1, /device:TPU:25, one launch (start us, length us, event | category | flops | bytes accessed | tf_op | source)
XLA Modules:
  0.0 89.3 jit_solution(16281207964331320023)
XLA Ops:
  0.0 0.5 fusion
  0.6 0.8 pad_maximum_fusion.sine_part
  1.4 0.1 copy.19
  1.5 0.8 copy.20.cosine
  2.2 84.8 %shard_map.145 = bf16[256,2048]{1,0:T(8,128)(2,1)} custom-call(bf16[256,2048]{1,0:T(8,128)(2,1)} %tokens.1, f32[1,2048]{1,0:T(1,128)} %bitcast.6, bf16[256,256]{1,0:T(8,128)(2,1)} %wk.1, bf16[256,256]{1,0:T(8,128)(2,1)} %wv.1, bf16[256,256]{1,0:T(8,128)(2,1)} %wq.1, bf16[256,256]{1,0:T(8,128)(2,1)} %wf.1, bf16[256,256]{1,0:T(8,128)(2,1)} %wi.1, ...), custom_call_target="tpu_custom_call" | custom-call | tf_op jit(solution)/shard_map/pallas_call | solution.py:637
  87.0 2.3 %copy.22 = bf16[256,2048]{1,0:T(8,128)(2,1)} copy(bf16[256,2048]{1,0:T(8,128)(2,1)} %shard_map.145) | data formatting | bytes 2097152
  (3 shorter events, 0.0 us)

commit v2 on v1

--- a/solution.py
+++ b/solution.py
@@ -309,15 +309,18 @@
 
 def fused_kernel(
     n, tps, span,
-    tokens, gain, wk, wv, wq, wf, wi, wr, rec_out, att_out, gap, shift, rec_gain, att_gain, cosine, sine_part,
+    tokens_far, wk, wv, wq, wf, wi, wr, rec_out, att_out, gain, gap, shift, rec_gain, att_gain, rates,
     lam, out,
     buf, xn, acc, wo, mix, kv, kv_prev, st, st_prev, total,
-    ssem, rsem, wo_s, wo_r, mix_s, mix_r, ex_s, ex_r,
+    tokens, near, cosine, sine_part,
+    ssem, rsem, wo_s, wo_r, mix_s, mix_r, ex_s, ex_r, in_sem,
 ):
     weights = (wk, wv, wq, wf, wi, wr)
     chunks = len(weights)
     rows, width = tokens.shape
     depth, cols = wk.shape
+    loads = [pltpu.make_async_copy(tokens_far, tokens, in_sem.at[0])]
+    loads += [pltpu.make_async_copy(w, near.at[c], in_sem.at[1 + c]) for c, w in enumerate(weights)]
     me = lax.axis_index("sp")
     t = lax.axis_index("tp")
     up = (1 - me % 2)
@@ -338,6 +341,8 @@
     to_right, to_left = {"sp": right}, {"sp": left}
     to_partner, to_across = {"tp": partner}, {"tp": across}
 
+    for load in loads:
+        load.start()
     barrier = pltpu.get_barrier_semaphore()
     for target in (to_right, to_left, to_partner, to_across):
         pl.semaphore_signal(barrier, inc=1, device_id=target, device_id_type=MESH)
@@ -388,6 +393,7 @@
         )
 
     outs_w = (rec_out, att_out)
+    outs_near = [pltpu.make_async_copy(outs_w[k], wo.at[3, k], in_sem.at[7 + k]) for k in range(2)]
 
     def wo_copy(k, part):
         src = outs_w[part] if k < 2 else wo.at[1, part]
@@ -403,7 +409,9 @@
     for part in range(2):
         wo_copy(1, part).start()
         wo_copy(0, part).start()
-
+        outs_near[part].start()
+
+    loads[0].wait()
     values = tokens[...].astype(F32)
     mean_sq = jnp.mean(values * values, axis=-1, keepdims=True)
     normed = (values * lax.rsqrt(mean_sq + RECUR_EPSILON) * gain[...]).astype(BF16)
@@ -411,7 +419,15 @@
         xn[k] = normed[:, k * depth : (k + 1) * depth]
     mine = xn[me]
     for c in range(chunks):
-        acc[c] = nn(mine, weights[c][...])
+        loads[1 + c].wait()
+        acc[c] = nn(mine, near[c])
+
+    start = me - jnp.maximum(me - stage, 0)
+    position = (lax.broadcasted_iota(jnp.int32, (rows, CUT), 0) + start * rows).astype(F32)
+    angles = position * rates[...]
+    signs = jnp.where(lax.broadcasted_iota(jnp.int32, (rows, CUT), 1) % PAIR < PAIR // 2, -1.0, 1.0)
+    cosine[...] = jnp.cos(angles)
+    sine_part[...] = jnp.sin(angles) * signs
 
     def project(way, hop, c):
         ring(way, hop, c).wait_recv()
@@ -515,6 +531,7 @@
             decay = decay + cum[CUT - 1 : CUT]
 
     for part in range(2):
+        outs_near[part].wait()
         wo_copy(0, part).wait_recv()
         wo_copy(2, part).wait_recv()
 
@@ -571,33 +588,29 @@
     tile = 2 * cols
     tiles = width // tile
 
-    def add(k, part, first=False):
-        source = outs_w[part] if k == 3 else wo.at[k, part]
-        left_side = mix[k, part]
+    def add(*terms, first=False, last=False):
         for j in range(tiles):
             span_cols = slice(j * tile, (j + 1) * tile)
-            product = nn(left_side, source[:, span_cols])
-            total[:, span_cols] = product if first else total[:, span_cols] + product
-
-    add(3, 0, True)
+            product = sum(nn(mix[k, part], wo[k, part, :, span_cols]) for k, part in terms)
+            if not first:
+                product = product + total[:, span_cols]
+            if last:
+                out[:, span_cols] = product.astype(BF16)
+            else:
+                total[:, span_cols] = product
+
     mix_copy(1, 0).wait_recv()
     mix_copy(2, 0).start()
-    add(3, 1)
     mix_copy(0, 0).wait_recv()
-    add(0, 0)
-    add(1, 0)
+    add((3, 0), (3, 1), (0, 0), (1, 0), first=True)
     mix_copy(2, 0).wait_recv()
-    add(2, 0)
     mix_copy(0, 1).wait_recv()
-    add(0, 1)
+    add((2, 0), (0, 1))
     mix_copy(1, 1).wait_recv()
     mix_copy(2, 1).start()
-    add(1, 1)
+    add((1, 1))
     mix_copy(2, 1).wait_recv()
-    left_side = mix[2, 1]
-    for j in range(tiles):
-        span_cols = slice(j * tile, (j + 1) * tile)
-        out[:, span_cols] = (total[:, span_cols] + nn(left_side, wo[2, 1, :, span_cols])).astype(BF16)
+    add((2, 1), last=True)
 
     for hop in range(1, top + 1):
         for way in range(2):
@@ -622,34 +635,31 @@
 ):
     rows, width = tokens_in.shape
     depth, cols = att_key_weight.shape
-    me = lax.axis_index("sp")
-    half = span // 2
-    first_dev = jnp.maximum(0, (me + half) // span * span - half)
-    positions = ((me - first_dev) * rows + jnp.arange(rows, dtype=jnp.int32)).astype(F32)
     half_width = PAIR // 2
     frequency = 1.0 / ROTARY_BASE ** (jnp.arange(half_width, dtype=F32) / half_width)
-    angles = positions[:, None] * frequency[None, :]
-    cosine = jnp.tile(jnp.cos(angles), (1, 4))
-    sine_one = jnp.sin(angles)
-    sine_part = jnp.concatenate([-sine_one, sine_one, -sine_one, sine_one], axis=1)
+    rates = jnp.tile(frequency, CUT // half_width)[None]
     heads = cols // CUT
     vmem = pl.BlockSpec(memory_space=pltpu.VMEM)
     return pl.pallas_call(
         functools.partial(fused_kernel, n, tps, span),
         out_shape=jax.ShapeDtypeStruct((rows, width), BF16),
-        in_specs=[vmem] * 16 + [pl.BlockSpec(memory_space=pltpu.SMEM)],
+        in_specs=[pl.BlockSpec(memory_space=pltpu.HBM)] * 9 + [vmem] * 6 + [pl.BlockSpec(memory_space=pltpu.SMEM)],
         out_specs=vmem,
         scratch_shapes=[
             pltpu.VMEM((n, 6, depth, cols), BF16),
             pltpu.VMEM((n, rows, depth), BF16),
             pltpu.VMEM((6, rows, cols), F32),
-            pltpu.VMEM((3, 2, cols, width), BF16),
+            pltpu.VMEM((4, 2, cols, width), BF16),
             pltpu.VMEM((4, 2, rows, cols), BF16),
             pltpu.VMEM((2, rows, cols), BF16),
             pltpu.VMEM((2, rows, cols), BF16),
             pltpu.VMEM((heads, CUT, CUT), F32),
             pltpu.VMEM((heads, CUT, CUT), F32),
             pltpu.VMEM((rows, width), F32),
+            pltpu.VMEM((rows, width), BF16),
+            pltpu.VMEM((6, depth, cols), BF16),
+            pltpu.VMEM((rows, CUT), F32),
+            pltpu.VMEM((rows, CUT), F32),
             pltpu.SemaphoreType.DMA((2, n // 2, 6)),
             pltpu.SemaphoreType.DMA((n, 6)),
             pltpu.SemaphoreType.DMA((3, 2)),
@@ -658,12 +668,13 @@
             pltpu.SemaphoreType.DMA((3, 2)),
             pltpu.SemaphoreType.DMA((3,)),
             pltpu.SemaphoreType.DMA((3,)),
+            pltpu.SemaphoreType.DMA((9,)),
         ],
-        compiler_params=pltpu.CompilerParams(collective_id=0, has_side_effects=True, vmem_limit_bytes=56 << 20),
+        compiler_params=pltpu.CompilerParams(collective_id=0, has_side_effects=True, vmem_limit_bytes=60 << 20),
     )(
-        tokens_in, norm_gain[None], att_key_weight, att_value_weight, att_query_weight,
+        tokens_in, att_key_weight, att_value_weight, att_query_weight,
         rec_forget_weight, rec_input_weight, rec_query_weight, recurrence_output_weight, out_att_weight,
-        floor_gap[None], decay_shift, rec_gain[None], att_gain[None], cosine, sine_part, lambda_head,
+        norm_gain[None], floor_gap[None], decay_shift, rec_gain[None], att_gain[None], rates, lambda_head,
     )
 
 

time: 89.5 us -> 86.9 us (0.971)
  other arithmetic: 1.38 us -> 0.01 us
  Pallas kernels: 84.8 us -> 83.8 us
    pallas_call x1, Pallas kernels: 84.8 us -> 83.8 us  [per_device_fused(): pl.pallas_call(functools.partial(fused_kernel, n, tps, span), out_shape=j...]
where the time goes in v2:
time: 86.9 us; the launch traced here: 86.7 us
  Pallas kernels  83.8 us (96%)
  local copies, waits for them, and re-layouts  2.91 us (3%)
    pallas_call x1, Pallas kernels, per_device_fused(): pl.pallas_call(functools.partial(fused_kernel, n, tps, span), out_shape=j...  83.8 us
    unnamed x1, local copies, waits for them, and re-layouts  2.3 us

profile of v2, /device:TPU:25, one launch (start us, length us, event | category | flops | bytes accessed | tf_op | source)
XLA Modules:
  0.0 86.7 jit_solution(9809524213052256566)
XLA Ops:
  0.0 0.6 broadcast_in_dim_tile.3.rates
  0.6 83.8 %shard_map.145 = bf16[256,2048]{1,0:T(8,128)(2,1)} custom-call(bf16[256,2048]{1,0:T(8,128)(2,1)} %tokens_far.1, bf16[256,256]{1,0:T(8,128)(2,1)} %wk.1, bf16[256,256]{1,0:T(8,128)(2,1)} %wv.1, bf16[256,256]{1,0:T(8,128)(2,1)} %wq.1, bf16[256,256]{1,0:T(8,128)(2,1)} %wf.1, bf16[256,256]{1,0:T(8,128)(2,1)} %wi.1, bf16[256,256]{1,0:T(8,128)(2,1)} %wr.1, ...), custom_call_target="tpu_custom_call" | custom-call | tf_op jit(solution)/shard_map/pallas_call | solution.py:643
  84.4 2.3 %copy.17 = bf16[256,2048]{1,0:T(8,128)(2,1)} copy(bf16[256,2048]{1,0:T(8,128)(2,1)} %shard_map.145) | data formatting | bytes 2097152
  (2 shorter events, 0.0 us)

commit v3 on v2

--- a/solution.py
+++ b/solution.py
@@ -315,7 +315,7 @@
     tokens, near, cosine, sine_part,
     ssem, rsem, wo_s, wo_r, mix_s, mix_r, ex_s, ex_r, in_sem,
 ):
-    weights = (wk, wv, wq, wf, wi, wr)
+    weights = (wk, wf, wq, wv, wi, wr)
     chunks = len(weights)
     rows, width = tokens.shape
     depth, cols = wk.shape
@@ -447,7 +447,7 @@
     @pl.when(jnp.logical_not(is_recv))
     def _():
         kv_prev[...] = jnp.zeros(kv_prev.shape, BF16)
-        st_prev[...] = jnp.zeros(st_prev.shape, F32)
+        st_prev[...] = jnp.zeros(st_prev.shape, BF16)
 
     def ex_copy(k):
         src, dst = ((kv.at[0], kv_prev.at[0]), (kv.at[1], kv_prev.at[1]), (st, st_prev))[k]
@@ -470,10 +470,17 @@
         ex_copy(0).start()
 
     project(1, top, 3)
+    kv[1] = acc[3].astype(BF16)
+
+    @pl.when(is_send)
+    def _():
+        ex_copy(1).start()
+
+    project(0, top, 1)
     cums, keys = [], []
     for h in range(heads):
         lanes = slice(h * CUT, (h + 1) * CUT)
-        forget = acc[3, :, lanes].astype(BF16).astype(F32)
+        forget = acc[1, :, lanes].astype(BF16).astype(F32)
         key = gap[:, lanes] * (1.0 / (1.0 + jnp.exp(forget)))
         high, low = halves(jnp.log(1.0 - key))
         for b in range(blocks):
@@ -481,13 +488,6 @@
             s_high, s_low = halves(jnp.broadcast_to(shift[h : h + 1, part], (CUT, CUT)))
             cums.append(nn(ones, high[part]) + nn(ones, low[part]) + nt(ones, s_high) + nt(ones, s_low))
             keys.append(key[part])
-
-    project(0, top, 1)
-    kv[1] = acc[1].astype(BF16)
-
-    @pl.when(is_send)
-    def _():
-        ex_copy(1).start()
 
     project(1, top, 4)
     fresh, inputs = [], []
@@ -502,7 +502,7 @@
             fresh.append(own)
             own = own * jnp.exp(end) + tn(inp, to_end)
             inputs.append(inp)
-        st[h] = own
+        st[h] = own.astype(BF16)
 
     @pl.when(is_send)
     def _():
@@ -558,7 +558,7 @@
         for b in range(blocks):
             i = h * blocks + b
             past, decay = pasts[i]
-            came = (st_prev[h] * jnp.exp(decay)).astype(BF16)
+            came = (st_prev[h].astype(F32) * jnp.exp(decay)).astype(BF16)
             raw = raws[i] + nt(past.astype(BF16), came)
             mean_sq = jnp.mean(raw * raw, axis=-1, keepdims=True)
             mix[3, 0, b * CUT : (b + 1) * CUT, lanes] = (
@@ -653,8 +653,8 @@
             pltpu.VMEM((4, 2, rows, cols), BF16),
             pltpu.VMEM((2, rows, cols), BF16),
             pltpu.VMEM((2, rows, cols), BF16),
-            pltpu.VMEM((heads, CUT, CUT), F32),
-            pltpu.VMEM((heads, CUT, CUT), F32),
+            pltpu.VMEM((heads, CUT, CUT), BF16),
+            pltpu.VMEM((heads, CUT, CUT), BF16),
             pltpu.VMEM((rows, width), F32),
             pltpu.VMEM((rows, width), BF16),
             pltpu.VMEM((6, depth, cols), BF16),

time: 86.9 us -> 85.5 us (0.984)
  Pallas kernels: 83.8 us -> 82.4 us
    pallas_call x1, Pallas kernels: 83.8 us -> 82.4 us  [per_device_fused(): pl.pallas_call(functools.partial(fused_kernel, n, tps, span), out_shape=j...]
where the time goes in v3:
time: 85.5 us; the launch traced here: 85.3 us
  Pallas kernels  82.4 us (96%)
  local copies, waits for them, and re-layouts  2.91 us (3%)
    pallas_call x1, Pallas kernels, per_device_fused(): pl.pallas_call(functools.partial(fused_kernel, n, tps, span), out_shape=j...  82.4 us
    unnamed x1, local copies, waits for them, and re-layouts  2.3 us

profile of v3, /device:TPU:25, one launch (start us, length us, event | category | flops | bytes accessed | tf_op | source)
XLA Modules:
  0.0 85.3 jit_solution(15288209011513364921)
XLA Ops:
  0.0 0.6 broadcast_in_dim_tile.3.rates
  0.6 82.4 %shard_map.145 = bf16[256,2048]{1,0:T(8,128)(2,1)} custom-call(bf16[256,2048]{1,0:T(8,128)(2,1)} %tokens_far.1, bf16[256,256]{1,0:T(8,128)(2,1)} %wk.1, bf16[256,256]{1,0:T(8,128)(2,1)} %wv.1, bf16[256,256]{1,0:T(8,128)(2,1)} %wq.1, bf16[256,256]{1,0:T(8,128)(2,1)} %wf.1, bf16[256,256]{1,0:T(8,128)(2,1)} %wi.1, bf16[256,256]{1,0:T(8,128)(2,1)} %wr.1, ...), custom_call_target="tpu_custom_call" | custom-call | tf_op jit(solution)/shard_map/pallas_call | solution.py:643
  83.0 2.3 %copy.17 = bf16[256,2048]{1,0:T(8,128)(2,1)} copy(bf16[256,2048]{1,0:T(8,128)(2,1)} %shard_map.145) | data formatting | bytes 2097152
  (2 shorter events, 0.0 us)
